TPU v7x, 128 devices: a whole 4x4x4 slice. The times are simulated.
128 devices in a mesh: sp: 16 (over z, y), tp: 8 (over x, core).
Axes of the slice: x: 4, y: 4, z: 4, core: 2. Of those that a mesh axis runs over, the one named last changes fastest.
Arguments:
- hidden: bfloat16 [6144, 4096], P('sp', 'tp'), may hold values from -6 to 6
- doc_ids: int32 [6144], P('sp'), may hold values from 0 to 7, never falling along the last dimension, each value on 1 to 1536 neighbouring positions
- norm_gain: float32 [3, 4096], replicated, may hold values from 0.1 to 1.9
- w_value: bfloat16 [3, 4096, 2048], P(None, 'sp', 'tp'), may hold values from -0.09375 to 0.09375
- w_gate: bfloat16 [3, 4096, 2048], P(None, 'sp', 'tp'), may hold values from -0.09375 to 0.09375
- conv_taps: float32 [3, 31, 2048], P(None, None, 'tp'), may hold values from -1 to 1
- conv_bias: float32 [3, 2048], P(None, 'tp'), may hold values from -3 to 3
- chan_gain: float32 [3, 2048], P(None, 'tp'), may hold values from 0.1 to 1.9
- chan_bias: float32 [3, 2048], P(None, 'tp'), may hold values from -3 to 3
- w_out: bfloat16 [3, 2048, 4096], P(None, 'sp', 'tp'), may hold values from -0.125 to 0.125
Outputs:
- result: bfloat16 [6144, 4096], P('sp', 'tp')
Inputs may be any that keep to these rules, and one draw needn't show every extreme that they name: `doc_ids`: document numbers never fall along the sequence; each document has 1 to 1536 positions and one has exactly that many.
All inputs are finite; a program needn't handle non-finite values.
Results may differ from a plain program's by a relative error of at most 0.013.
Values may be sent and summed in bfloat16 or wider, within the bound.
No kernel may reach another device: no remote copies, remote signals or barrier semaphores. Data moves between devices by JAX's collectives and lax.ppermute only.
A program may use at most 128 MiB of HBM per device.

v0:
```python
import jax
import jax.numpy as jnp
from jax import lax
from jax.sharding import PartitionSpec as P

LAYERS = 3


def side_by_side(arrays, axis, dim, along):
    ends, at = ([], 0)
    for a in arrays[:-1]:
        at += a.shape[along]
        ends.append(at)
    both = jnp.concatenate(arrays, axis=along)
    return tuple(jnp.split(lax.all_gather(both, axis, axis=dim, tiled=True), ends, axis=along))


def from_behind(shard, axis, by):
    size = lax.axis_size(axis)
    pairs = [(i, i + by) for i in range(size) if 0 <= i + by < size]
    return lax.ppermute(shard, axis, pairs)


def sent_to_all(shard, axis):
    size = lax.axis_size(axis)
    return lax.all_to_all(
        jnp.broadcast_to(shard[None], (size, *shard.shape)), axis, 0, 0, tiled=True
    )


def of_everyone(shard, axis):
    return sent_to_all(shard, axis).sum(axis=0)


def in_one(arrays, axis):
    ends = [0]
    for a in arrays:
        ends.append(ends[-1] + a.size)
    total = of_everyone(jnp.concatenate([a.ravel() for a in arrays]), axis)
    return tuple((total[b:e].reshape(a.shape) for a, b, e in zip(arrays, ends, ends[1:])))


def joined_along(blocks, dim):
    blocks = jnp.moveaxis(blocks, 0, dim)
    shape = blocks.shape
    return blocks.reshape(*shape[:dim], shape[dim] * shape[dim + 1], *shape[dim + 2 :])


def gather_directly(shard, axis, dim):
    return joined_along(sent_to_all(shard, axis), dim)


def per_device(
    hidden, doc_ids, norm_gain, w_value, w_gate, conv_taps, conv_bias, chan_gain, chan_bias, w_out
):
    width = conv_taps.shape[1]
    length = hidden.shape[0]
    chan_local = w_value.shape[2]
    chan_total = chan_local * lax.axis_size("tp")
    seg_own = doc_ids + 1
    value_all, gate_all, out_all = (
        *side_by_side((w_value, w_gate), "sp", 1, 0),
        lax.all_gather(w_out, "sp", axis=1, tiled=True),
    )
    state = hidden
    for layer in range(LAYERS):
        whole = lax.all_gather(state, "tp", axis=1, tiled=True)
        xwhole = whole.astype(jnp.float32)
        scale = lax.rsqrt(jnp.mean(xwhole * xwhole, axis=-1, keepdims=True) + 1e-06)
        normed = (xwhole * scale * norm_gain[layer]).astype(jnp.bfloat16)
        value = jnp.dot(normed, value_all[layer], preferred_element_type=jnp.float32)
        gate = jnp.dot(normed, gate_all[layer], preferred_element_type=jnp.float32)
        glu = (value * jax.nn.sigmoid(gate)).astype(jnp.bfloat16)
        halo_glu, halo_seg = from_behind(
            (glu[length - (width - 1) :], seg_own[length - (width - 1) :]), "sp", 1
        )
        extended = jnp.concatenate([halo_glu, glu], axis=0).astype(jnp.float32)
        seg_ext = jnp.concatenate([halo_seg.astype(jnp.int32), seg_own], axis=0)
        taps = conv_taps[layer]
        conv = jnp.zeros((length, chan_local), jnp.float32) + conv_bias[layer]
        for index in range(width):
            keep = (seg_ext[index : index + length] == seg_own)[:, None]
            conv = conv + jnp.where(keep, extended[index : index + length] * taps[index], 0.0)
        total, square = in_one((jnp.sum(conv, axis=-1), jnp.sum(conv * conv, axis=-1)), "tp")
        mean_val = (total / chan_total)[:, None]
        var_val = (square / chan_total)[:, None] - mean_val * mean_val
        mixed = jax.nn.silu(
            (conv - mean_val) * lax.rsqrt(var_val + 1e-05) * chan_gain[layer] + chan_bias[layer]
        ).astype(jnp.bfloat16)
        mixed_all = gather_directly(mixed, "tp", 1)
        branch = jnp.dot(mixed_all, out_all[layer], preferred_element_type=jnp.float32)
        state = (state.astype(jnp.float32) + branch).astype(jnp.bfloat16)
    return state


def solution(mesh):
    placed = (
        P("sp", "tp"),
        P("sp"),
        P(),
        P(None, "sp", "tp"),
        P(None, "sp", "tp"),
        P(None, None, "tp"),
        P(None, "tp"),
        P(None, "tp"),
        P(None, "tp"),
        P(None, "sp", "tp"),
    )
    return jax.shard_map(
        per_device, mesh=mesh, in_specs=placed, out_specs=P("sp", "tp"), check_vma=False
    )
```

profile of v0, /device:TPU:32, one launch (start us, length us, event | category | flops | bytes accessed | tf_op | source)
XLA Modules:
  0.0 367.8 jit_solution(13401062077988971587)
XLA Ops:
  6.6 0.7 all-gather.6.cloned.1.call-update
  7.3 2.1 pad_maximum_fusion
  9.5 0.7 all-gather.10.cloned.1.call-update
  10.3 3.5 collective-permute-start
  13.9 3.9 %collective-permute-done = s32[30]{0:T(128)S(1)} collective-permute-done((s32[30]{0:T(128)S(1)}, s32[30]{0:T(128)S(1)}, u32[]{:S(2)}, u32[]{:S(2)}) %collective-permute-start) | collective-permute-done | bytes 152 | tf_op jit(solution)/shard_map/ppermute | solution.py:21
  18.0 20.7 %all-gather.6.cloned.1.call-done = bf16[384,4096]{1,0:T(8,128)(2,1)} async-done(((bf16[384,512]{1,0:T(8,128)(2,1)}), bf16[384,4096]{1,0:T(8,128)(2,1)}) %all-gather.6.cloned.1.call-update) | async-done | bytes 3145744 | tf_op jit(solution)/shard_map/all_gather | solution.py:67
  38.8 2.7 fusion
  41.5 89.1 %all-gather.8.cloned.1.call-done = bf16[6,4096,256]{2,1,0:T(8,128)(2,1)} async-done(((bf16[6,256,256]{2,1,0:T(8,128)(2,1)}), bf16[6,4096,256]{2,1,0:T(8,128)(2,1)}) %all-gather.8.cloned.1.call-update) | async-done | bytes 12582928 | tf_op jit(solution)/shard_map/all_gather | solution.py:15
  130.6 2.6 fusion.38
  133.2 2.6 fusion.41
  135.9 2.2 collective-permute-start.1
  138.2 5.4 %collective-permute-done.1 = bf16[30,256]{1,0:T(8,128)(2,1)S(1)} collective-permute-done((bf16[30,256]{1,0:T(8,128)(2,1)S(1)}, bf16[30,256]{1,0:T(8,128)(2,1)S(1)}, u32[]{:S(2)}, u32[]{:S(2)}) %collective-permute-start.1) | collective-permute-done | bytes 15392 | tf_op jit(solution)/shard_map/ppermute | solution.py:21
  143.7 3.4 fusion.233
  147.1 0.6 broadcast_in_dim.604
  147.8 4.3 %all-to-all-start = ((f32[8,1,768]{2,1,0:T(1,128)}), f32[8,1,768]{2,1,0:T(1,128)S(1)}, u32[]{:S(2)}, u32[]{:S(2)}) async-start(f32[8,1,768]{2,1,0:T(1,128)} %broadcast_in_dim.604), calls=%async_computation | async-start | bytes 49152 | tf_op jit(solution)/shard_map/all_to_all | solution.py:26
  152.0 5.4 %all-to-all-done = f32[8,1,768]{2,1,0:T(1,128)S(1)} async-done(((f32[8,1,768]{2,1,0:T(1,128)}), f32[8,1,768]{2,1,0:T(1,128)S(1)}, u32[]{:S(2)}, u32[]{:S(2)}) %all-to-all-start) | async-done | bytes 24608 | tf_op jit(solution)/shard_map/all_to_all | solution.py:26
  157.5 0.2 multiply_convert_fusion.2
  157.7 0.2 copy.18
  157.9 1.3 broadcast_in_dim.605
  159.2 3.6 all-to-all-start.1
  162.8 31.0 %all-gather.10.cloned.1.call-done = bf16[3,2048,512]{2,1,0:T(8,128)(2,1)} async-done(((bf16[3,128,512]{2,1,0:T(8,128)(2,1)}), bf16[3,2048,512]{2,1,0:T(8,128)(2,1)}) %all-gather.10.cloned.1.call-update) | async-done | bytes 6291472 | tf_op jit(solution)/shard_map/all_gather | solution.py:63
  193.8 3.3 fusion.23
  197.2 27.5 %all-gather.12.cloned.1.call-done = bf16[384,4096]{1,0:T(8,128)(2,1)} async-done(((bf16[384,512]{1,0:T(8,128)(2,1)}), bf16[384,4096]{1,0:T(8,128)(2,1)}) %all-gather.12.cloned.1.call-update) | async-done | bytes 3145744 | tf_op jit(solution)/shard_map/all_gather | solution.py:67
  224.7 2.7 fusion.3
  227.6 2.7 fusion.36
  230.2 2.7 fusion.40
  232.9 3.4 collective-permute-start.2
  236.4 4.3 %collective-permute-done.2 = bf16[30,256]{1,0:T(8,128)(2,1)S(1)} collective-permute-done((bf16[30,256]{1,0:T(8,128)(2,1)S(1)}, bf16[30,256]{1,0:T(8,128)(2,1)S(1)}, u32[]{:S(2)}, u32[]{:S(2)}) %collective-permute-start.2) | collective-permute-done | bytes 15392 | tf_op jit(solution)/shard_map/ppermute | solution.py:21
  240.7 3.4 fusion.232
  244.2 8.3 %all_to_all.33 = f32[8,1,768]{2,1,0:T(1,128)S(1)} all-to-all(f32[8,1,768]{2,1,0:T(1,128)S(1)} %broadcast_in_dim.606), channel_id=1, replica_groups=mesh['sp'=16,'tp'=8] {'tp'}, dimensions={0} | all-to-all | bytes 49152 | tf_op jit(solution)/shard_map/all_to_all | solution.py:26
  252.5 0.2 multiply_convert_fusion.1
  252.8 0.2 copy.20
  252.9 0.1 broadcast_in_dim.607
  253.1 24.0 %all_to_all.34 = bf16[8,384,256]{1,2,0:T(8,128)(2,1)S(1)} all-to-all(bf16[8,384,256]{1,2,0:T(8,128)(2,1)S(1)} %broadcast_in_dim.607), channel_id=1, replica_groups=mesh['sp'=16,'tp'=8] {'tp'}, dimensions={0} | all-to-all | bytes 3145728 | tf_op jit(solution)/shard_map/all_to_all | solution.py:26
  277.1 3.4 fusion.22
  280.5 25.1 %all-gather.14.cloned.1.call-done = bf16[384,4096]{1,0:T(8,128)(2,1)} async-done(((bf16[384,512]{1,0:T(8,128)(2,1)}), bf16[384,4096]{1,0:T(8,128)(2,1)}) %all-gather.14.cloned.1.call-update) | async-done | bytes 3145744 | tf_op jit(solution)/shard_map/all_gather | solution.py:67
  305.6 2.7 fusion.6
  308.4 2.7 fusion.34
  311.1 2.7 fusion.39
  313.8 3.4 collective-permute-start.3
  317.2 4.3 %collective-permute-done.3 = bf16[30,256]{1,0:T(8,128)(2,1)S(1)} collective-permute-done((bf16[30,256]{1,0:T(8,128)(2,1)S(1)}, bf16[30,256]{1,0:T(8,128)(2,1)S(1)}, u32[]{:S(2)}, u32[]{:S(2)}) %collective-permute-start.3) | collective-permute-done | bytes 15392 | tf_op jit(solution)/shard_map/ppermute | solution.py:21
  321.6 3.4 fusion.231
  325.1 8.3 %all_to_all.35 = f32[8,1,768]{2,1,0:T(1,128)S(1)} all-to-all(f32[8,1,768]{2,1,0:T(1,128)S(1)} %broadcast_in_dim.608), channel_id=1, replica_groups=mesh['sp'=16,'tp'=8] {'tp'}, dimensions={0} | all-to-all | bytes 49152 | tf_op jit(solution)/shard_map/all_to_all | solution.py:26
  333.4 0.2 multiply_convert_fusion
  333.6 0.2 copy.22
  333.8 0.1 broadcast_in_dim.609
  333.9 24.0 %all_to_all.36 = bf16[8,384,256]{1,2,0:T(8,128)(2,1)S(1)} all-to-all(bf16[8,384,256]{1,2,0:T(8,128)(2,1)S(1)} %broadcast_in_dim.609), channel_id=1, replica_groups=mesh['sp'=16,'tp'=8] {'tp'}, dimensions={0} | all-to-all | bytes 3145728 | tf_op jit(solution)/shard_map/all_to_all | solution.py:26
  358.0 3.4 fusion.21
  (67 shorter events, 1.3 us)
Async XLA Ops:
  6.5 3.7 copy-start.8
  6.5 7.2 %copy-start.9 = (f32[3,256]{1,0:T(4,128)S(1)}, f32[3,256]{1,0:T(4,128)}, u32[]{:S(2)}) copy-start(f32[3,256]{1,0:T(4,128)} %param.16) | copy-start | bytes 9220
  6.5 7.3 %copy-start.6 = (f32[3,31,256]{2,1,0:T(8,128)S(1)}, f32[3,31,256]{2,1,0:T(8,128)}, u32[]{:S(2)}) copy-start(f32[3,31,256]{2,1,0:T(8,128)} %param.15) | copy-start | bytes 285700
  6.5 7.3 %copy-start.7 = (f32[3,4096]{1,0:T(4,128)S(1)}, f32[3,4096]{1,0:T(4,128)}, u32[]{:S(2)}) copy-start(f32[3,4096]{1,0:T(4,128)} %param.12) | copy-start | bytes 147460
  6.5 7.4 %copy-start.10 = (f32[3,256]{1,0:T(4,128)S(1)}, f32[3,256]{1,0:T(4,128)}, u32[]{:S(2)}) copy-start(f32[3,256]{1,0:T(4,128)} %param.17) | copy-start | bytes 9220
  6.5 32.2 %all-gather.6.cloned.1.call-start = ((), (), s32[]{:S(2)}) async-start(), calls=%async_computation.6 | async-start | bytes 3538944 | tf_op jit(solution)/shard_map/all_gather | solution.py:67
  7.3 123.3 %all-gather.8.cloned.1.call-start = ((), (), s32[]{:S(2)}) async-start(), calls=%async_computation.7 | async-start | bytes 13369344 | tf_op jit(solution)/shard_map/all_gather | solution.py:15
  9.5 184.3 %all-gather.10.cloned.1.call-start = ((), (), s32[]{:S(2)}) async-start(), calls=%async_computation.8 | async-start | bytes 6684672 | tf_op jit(solution)/shard_map/all_gather | solution.py:63
  10.3 7.6 %collective-permute-start = (s32[30]{0:T(128)S(1)}, s32[30]{0:T(128)S(1)}, u32[]{:S(2)}, u32[]{:S(2)}) collective-permute-start(s32[30]{0:T(128)S(1)} %slice.999), channel_id=1, source_target_pairs={{0,8},{8,16},{16,24},{24,32},{32,40},{40,48},{48,56},{56,64},{64,7... | collective-permute-start | bytes 368 | tf_op jit(solution)/shard_map/ppermute | solution.py:21
  38.8 91.8 %copy-start = (bf16[384,4096]{1,0:T(8,128)(2,1)S(1)}, bf16[384,4096]{1,0:T(8,128)(2,1)}, u32[]{:S(2)}) copy-start(bf16[384,4096]{1,0:T(8,128)(2,1)} %all-gather.6.cloned.1.call-done) | copy-start | bytes 9437188
  135.9 7.7 %collective-permute-start.1 = (bf16[30,256]{1,0:T(8,128)(2,1)S(1)}, bf16[30,256]{1,0:T(8,128)(2,1)S(1)}, u32[]{:S(2)}, u32[]{:S(2)}) collective-permute-start(bf16[30,256]{1,0:T(8,128)(2,1)S(1)} %slice.1247), channel_id=1, source_target_pairs={{0,8},{8,16},{16,24},{24,32},{32,40},{40,48},{48,56},{56,64},{64,7... | collective-permute-start | bytes 46088 | tf_op jit(solution)/shard_map/ppermute | solution.py:21
  143.7 8.3 %copy-start.11 = (f32[3,256]{1,0:T(4,128)S(1)}, f32[3,256]{1,0:T(4,128)}, u32[]{:S(2)}) copy-start(f32[3,256]{1,0:T(4,128)} %param.18) | copy-start | bytes 9220
  147.1 46.7 %copy-start.3 = (bf16[384,512]{1,0:T(8,128)(2,1)S(1)}, bf16[384,512]{1,0:T(8,128)(2,1)}, u32[]{:S(2)}) copy-start(bf16[384,512]{1,0:T(8,128)(2,1)} %param.10) | copy-start | bytes 1179652
  147.8 9.7 %all-to-all-start = ((f32[8,1,768]{2,1,0:T(1,128)}), f32[8,1,768]{2,1,0:T(1,128)S(1)}, u32[]{:S(2)}, u32[]{:S(2)}) async-start(f32[8,1,768]{2,1,0:T(1,128)} %broadcast_in_dim.604), calls=%async_computation | async-start | bytes 49152 | tf_op jit(solution)/shard_map/all_to_all | solution.py:26
  159.2 34.6 %all-to-all-start.1 = ((bf16[8,384,256]{1,2,0:T(8,128)(2,1)}), bf16[8,384,256]{1,2,0:T(8,128)(2,1)S(1)}, u32[]{:S(2)}, u32[]{:S(2)}) async-start(bf16[8,384,256]{1,2,0:T(8,128)(2,1)} %broadcast_in_dim.605), calls=%async_computation.1 | async-start | bytes 3145728 | tf_op jit(solution)/shard_map/all_to_all | solution.py:26
  162.8 62.0 %all-gather.12.cloned.1.call-start = ((), (), s32[]{:S(2)}) async-start(), calls=%async_computation.9 | async-start | bytes 3538944 | tf_op jit(solution)/shard_map/all_gather | solution.py:67
  197.1 108.5 %all-gather.14.cloned.1.call-start = ((), (), s32[]{:S(2)}) async-start(), calls=%async_computation.10 | async-start | bytes 3538944 | tf_op jit(solution)/shard_map/all_gather | solution.py:67
  224.7 2.8 copy-start.1
  232.9 7.7 %collective-permute-start.2 = (bf16[30,256]{1,0:T(8,128)(2,1)S(1)}, bf16[30,256]{1,0:T(8,128)(2,1)S(1)}, u32[]{:S(2)}, u32[]{:S(2)}) collective-permute-start(bf16[30,256]{1,0:T(8,128)(2,1)S(1)} %slice.1282), channel_id=1, source_target_pairs={{0,8},{8,16},{16,24},{24,32},{32,40},{40,48},{48,56},{56,64},{64,7... | collective-permute-start | bytes 46088 | tf_op jit(solution)/shard_map/ppermute | solution.py:21
  244.1 33.0 %copy-start.5 = (bf16[384,512]{1,0:T(8,128)(2,1)S(1)}, bf16[384,512]{1,0:T(8,128)(2,1)}, u32[]{:S(2)}) copy-start(bf16[384,512]{1,0:T(8,128)(2,1)} %fusion.23) | copy-start | bytes 1179652
  305.6 2.8 copy-start.2
  313.8 7.7 %collective-permute-start.3 = (bf16[30,256]{1,0:T(8,128)(2,1)S(1)}, bf16[30,256]{1,0:T(8,128)(2,1)S(1)}, u32[]{:S(2)}, u32[]{:S(2)}) collective-permute-start(bf16[30,256]{1,0:T(8,128)(2,1)S(1)} %slice.1317), channel_id=1, source_target_pairs={{0,8},{8,16},{16,24},{24,32},{32,40},{40,48},{48,56},{56,64},{64,7... | collective-permute-start | bytes 46088 | tf_op jit(solution)/shard_map/ppermute | solution.py:21
  325.0 32.9 %copy-start.4 = (bf16[384,512]{1,0:T(8,128)(2,1)S(1)}, bf16[384,512]{1,0:T(8,128)(2,1)}, u32[]{:S(2)}) copy-start(bf16[384,512]{1,0:T(8,128)(2,1)} %fusion.22) | copy-start | bytes 1179652
Sparse Core Ops, SparseCore 0:
  9.0 29.6 all-gather.5
  40.9 89.6 all-gather.7
  132.7 60.9 all-gather.9
  197.2 27.4 all-gather.11
  280.6 24.9 all-gather.13
where the time goes:
time: 369 us; the launch traced here: 368 us
  waiting for transfers between devices  218 us (59%)
  blocking collectives  64.6 us (18%)
  matrix products  26 us (7%)
  other arithmetic  21.8 us (6%)
  starting transfers between devices  20.5 us (6%)
  between operations  13.6 us (4%)
    all_gather x1, waiting for transfers between devices, side_by_side(): lax.all_gather(both, axis, axis=dim, tiled=True)  89.1 us
    all_gather x3, waiting for transfers between devices, per_device(): whole = lax.all_gather(state, 'tp', axis=1, tiled=True)  73.4 us
    all_to_all x4, blocking collectives, sent_to_all(): lax.all_to_all(jnp.broadcast_to(shard[None], (size, *shard.shape)), axis,...  64.6 us
    all_gather x1, waiting for transfers between devices, per_device(): lax.all_gather(w_out, 'sp', axis=1, tiled=True)  31 us
    ppermute x4, waiting for transfers between devices, from_behind(): return lax.ppermute(shard, axis, pairs)  18 us
    ppermute x4, starting transfers between devices, from_behind(): return lax.ppermute(shard, axis, pairs)  12.5 us
    reduce_sum x3, other arithmetic, per_device(): jnp.sum(conv, axis=-1)  10.2 us
    dot_general x3, matrix products, per_device(): jnp.dot(mixed_all, out_all[layer], preferred_element_type=jnp.float32)  10 us
  transfers between devices with their start and end apart: 11, of which 10 were waited for; matrix products, arithmetic and copies ran while one was open for 4% of the time, Pallas kernels for 0%

commit v1 on v0

--- a/solution.py
+++ b/solution.py
@@ -64,7 +64,8 @@
     )
     state = hidden
     for layer in range(LAYERS):
-        whole = lax.all_gather(state, "tp", axis=1, tiled=True)
+        part_next = lax.all_gather(state, "tp")
+        whole = jnp.concatenate(part_next, axis=1)
         xwhole = whole.astype(jnp.float32)
         scale = lax.rsqrt(jnp.mean(xwhole * xwhole, axis=-1, keepdims=True) + 1e-06)
         normed = (xwhole * scale * norm_gain[layer]).astype(jnp.bfloat16)

time: 369 us -> 382 us (1.035)
  local copies, waits for them, and re-layouts: 3.2 us -> 18.9 us
  waiting for transfers between devices: 218 us -> 211 us
    convert_element_type x0 -> x3, local copies, waits for them, and re-layouts: none -> 13.9 us  [the longest x2 11.1 us: per_device(): xwhole = whole.astype(jnp.float32)]
    convert_element_type x0 -> x3, other arithmetic: none -> 7.46 us  [per_device(): normed = (xwhole * scale * norm_gain[layer]).astype(jnp.bfloat16)]
    reduce_sum x3, other arithmetic: 8.2 us -> 4.12 us  [per_device(): scale = lax.rsqrt(jnp.mean(xwhole * xwhole, axis=-1, keepdims=True) + 1e-06)]
    all_gather x1, waiting for transfers between devices: 89.1 us -> 85.2 us  [side_by_side(): lax.all_gather(both, axis, axis=dim, tiled=True)]
  transfers between devices with their start and end apart: 11 -> 11, of which waited for: 10 -> 10; matrix products, arithmetic and copies ran while one was open for 4% -> 6% of each run, Pallas kernels for 0% -> 0%
where the time goes in v1:
time: 382 us; the launch traced here: 381 us
  waiting for transfers between devices  211 us (55%)
  blocking collectives  64.6 us (17%)
  matrix products  27 us (7%)
  other arithmetic  25.1 us (7%)
  starting transfers between devices  20.7 us (5%)
  local copies, waits for them, and re-layouts  18.9 us (5%)
  between operations  13.7 us (4%)
    all_gather x1, waiting for transfers between devices, side_by_side(): lax.all_gather(both, axis, axis=dim, tiled=True)  85.2 us
    all_gather x3, waiting for transfers between devices, per_device(): part_next = lax.all_gather(state, 'tp')  73.3 us
    all_to_all x4, blocking collectives, sent_to_all(): lax.all_to_all(jnp.broadcast_to(shard[None], (size, *shard.shape)), axis,...  64.6 us
    all_gather x1, waiting for transfers between devices, per_device(): lax.all_gather(w_out, 'sp', axis=1, tiled=True)  29.7 us
    ppermute x4, waiting for transfers between devices, from_behind(): return lax.ppermute(shard, axis, pairs)  16.1 us
    ppermute x4, starting transfers between devices, from_behind(): return lax.ppermute(shard, axis, pairs)  12.7 us
    convert_element_type x2, local copies, waits for them, and re-layouts, per_device(): xwhole = whole.astype(jnp.float32)  11.1 us
    reduce_sum x3, other arithmetic, per_device(): jnp.sum(conv, axis=-1)  10.2 us
  transfers between devices with their start and end apart: 11, of which 10 were waited for; matrix products, arithmetic and copies ran while one was open for 6% of the time, Pallas kernels for 0%

profile of v1, /device:TPU:32, one launch (start us, length us, event | category | flops | bytes accessed | tf_op | source)
XLA Modules:
  0.0 381.3 jit_solution(2066537456518714855)
XLA Ops:
  6.6 0.7 all-gather.13.cloned.1.call-update
  7.3 2.1 pad_maximum_fusion
  9.5 0.7 all-gather.11.cloned.1.call-update
  10.3 3.5 collective-permute-start
  14.5 0.6 fusion.231
  15.1 0.6 fusion.229
  15.7 2.1 collective-permute-done
  18.0 20.7 %all-gather.13.cloned.1.call-done = bf16[3072,512]{1,0:T(8,128)(2,1)} async-done(((bf16[384,512]{1,0:T(8,128)(2,1)}), bf16[3072,512]{1,0:T(8,128)(2,1)}) %all-gather.13.cloned.1.call-update) | async-done | bytes 3145744 | tf_op jit(solution)/shard_map/all_gather | solution.py:67
  38.7 2.7 fusion
  41.6 1.0 fusion.3
  42.5 2.8 copy.28
  45.4 85.2 %all-gather.9.cloned.1.call-done = bf16[6,4096,256]{2,1,0:T(8,128)(2,1)} async-done(((bf16[6,256,256]{2,1,0:T(8,128)(2,1)}), bf16[6,4096,256]{2,1,0:T(8,128)(2,1)}) %all-gather.9.cloned.1.call-update) | async-done | bytes 12582928 | tf_op jit(solution)/shard_map/all_gather | solution.py:15
  130.6 3.7 fusion.33
  134.4 2.6 fusion.36
  137.0 2.2 collective-permute-start.1
  139.3 5.5 %collective-permute-done.1 = bf16[30,256]{1,0:T(8,128)(2,1)S(1)} collective-permute-done((bf16[30,256]{1,0:T(8,128)(2,1)S(1)}, bf16[30,256]{1,0:T(8,128)(2,1)S(1)}, u32[]{:S(2)}, u32[]{:S(2)}) %collective-permute-start.1) | collective-permute-done | bytes 15392 | tf_op jit(solution)/shard_map/ppermute | solution.py:21
  145.0 3.4 fusion.222
  148.5 0.6 broadcast_in_dim.604
  149.1 4.3 %all-to-all-start = ((f32[8,1,768]{2,1,0:T(1,128)}), f32[8,1,768]{2,1,0:T(1,128)S(1)}, u32[]{:S(2)}, u32[]{:S(2)}) async-start(f32[8,1,768]{2,1,0:T(1,128)} %broadcast_in_dim.604), calls=%async_computation | async-start | bytes 49152 | tf_op jit(solution)/shard_map/all_to_all | solution.py:26
  153.3 5.4 %all-to-all-done = f32[8,1,768]{2,1,0:T(1,128)S(1)} async-done(((f32[8,1,768]{2,1,0:T(1,128)}), f32[8,1,768]{2,1,0:T(1,128)S(1)}, u32[]{:S(2)}, u32[]{:S(2)}) %all-to-all-start) | async-done | bytes 24608 | tf_op jit(solution)/shard_map/all_to_all | solution.py:26
  159.2 1.3 broadcast_in_dim.605
  160.5 3.6 all-to-all-start.1
  164.1 29.7 %all-gather.11.cloned.1.call-done = bf16[3,2048,512]{2,1,0:T(8,128)(2,1)} async-done(((bf16[3,128,512]{2,1,0:T(8,128)(2,1)}), bf16[3,2048,512]{2,1,0:T(8,128)(2,1)}) %all-gather.11.cloned.1.call-update) | async-done | bytes 6291472 | tf_op jit(solution)/shard_map/all_gather | solution.py:63
  193.8 3.3 fusion.18
  197.3 27.5 %all-gather.15.cloned.1.call-done = bf16[3072,512]{1,0:T(8,128)(2,1)} async-done(((bf16[384,512]{1,0:T(8,128)(2,1)}), bf16[3072,512]{1,0:T(8,128)(2,1)}) %all-gather.15.cloned.1.call-update) | async-done | bytes 3145744 | tf_op jit(solution)/shard_map/all_gather | solution.py:67
  224.8 5.6 %copy.31 = f32[8,384,512]{1,2,0:T(8,128)} copy(bf16[8,384,512]{2,1,0:T(8,128)(2,1)} %bitcast.212) | data formatting | bytes 9437184 | tf_op jit(solution)/shard_map/convert_element_type | solution.py:69
  230.4 0.7 multiply_reduce_fusion.1
  231.1 3.3 multiply_convert_fusion.1
  234.3 2.6 fusion.31
  237.0 2.6 fusion.35
  239.6 3.6 collective-permute-start.2
  243.3 4.1 %collective-permute-done.2 = bf16[30,256]{1,0:T(8,128)(2,1)S(1)} collective-permute-done((bf16[30,256]{1,0:T(8,128)(2,1)S(1)}, bf16[30,256]{1,0:T(8,128)(2,1)S(1)}, u32[]{:S(2)}, u32[]{:S(2)}) %collective-permute-start.2) | collective-permute-done | bytes 15392 | tf_op jit(solution)/shard_map/ppermute | solution.py:21
  247.5 3.4 fusion.221
  250.9 8.3 %all_to_all.33 = f32[8,1,768]{2,1,0:T(1,128)S(1)} all-to-all(f32[8,1,768]{2,1,0:T(1,128)S(1)} %broadcast_in_dim.606), channel_id=1, replica_groups=mesh['sp'=16,'tp'=8] {'tp'}, dimensions={0} | all-to-all | bytes 49152 | tf_op jit(solution)/shard_map/all_to_all | solution.py:26
  259.8 24.0 %all_to_all.34 = bf16[8,384,256]{1,2,0:T(8,128)(2,1)S(1)} all-to-all(bf16[8,384,256]{1,2,0:T(8,128)(2,1)S(1)} %broadcast_in_dim.607), channel_id=1, replica_groups=mesh['sp'=16,'tp'=8] {'tp'}, dimensions={0} | all-to-all | bytes 3145728 | tf_op jit(solution)/shard_map/all_to_all | solution.py:26
  283.8 3.4 fusion.17
  287.2 25.1 %all-gather.17.cloned.1.call-done = bf16[3072,512]{1,0:T(8,128)(2,1)} async-done(((bf16[384,512]{1,0:T(8,128)(2,1)}), bf16[3072,512]{1,0:T(8,128)(2,1)}) %all-gather.17.cloned.1.call-update) | async-done | bytes 3145744 | tf_op jit(solution)/shard_map/all_gather | solution.py:67
  312.3 5.6 %copy.34 = f32[8,384,512]{1,2,0:T(8,128)} copy(bf16[8,384,512]{2,1,0:T(8,128)(2,1)} %bitcast.214) | data formatting | bytes 9437184 | tf_op jit(solution)/shard_map/convert_element_type | solution.py:69
  317.9 0.7 multiply_reduce_fusion
  318.6 3.3 multiply_convert_fusion
  321.9 2.6 fusion.29
  324.5 2.6 fusion.34
  327.2 3.4 collective-permute-start.3
  330.6 4.3 %collective-permute-done.3 = bf16[30,256]{1,0:T(8,128)(2,1)S(1)} collective-permute-done((bf16[30,256]{1,0:T(8,128)(2,1)S(1)}, bf16[30,256]{1,0:T(8,128)(2,1)S(1)}, u32[]{:S(2)}, u32[]{:S(2)}) %collective-permute-start.3) | collective-permute-done | bytes 15392 | tf_op jit(solution)/shard_map/ppermute | solution.py:21
  335.0 3.4 fusion.220
  338.5 8.3 %all_to_all.35 = f32[8,1,768]{2,1,0:T(1,128)S(1)} all-to-all(f32[8,1,768]{2,1,0:T(1,128)S(1)} %broadcast_in_dim.608), channel_id=1, replica_groups=mesh['sp'=16,'tp'=8] {'tp'}, dimensions={0} | all-to-all | bytes 49152 | tf_op jit(solution)/shard_map/all_to_all | solution.py:26
  347.3 24.0 %all_to_all.36 = bf16[8,384,256]{1,2,0:T(8,128)(2,1)S(1)} all-to-all(bf16[8,384,256]{1,2,0:T(8,128)(2,1)S(1)} %broadcast_in_dim.609), channel_id=1, replica_groups=mesh['sp'=16,'tp'=8] {'tp'}, dimensions={0} | all-to-all | bytes 3145728 | tf_op jit(solution)/shard_map/all_to_all | solution.py:26
  371.4 3.4 fusion.16
  (98 shorter events, 3.3 us)
Async XLA Ops:
  6.5 3.7 copy-start.9
  6.5 7.2 %copy-start.8 = (f32[3,4096]{1,0:T(4,128)S(1)}, f32[3,4096]{1,0:T(4,128)}, u32[]{:S(2)}) copy-start(f32[3,4096]{1,0:T(4,128)} %param.12) | copy-start | bytes 147460
  6.5 7.4 %copy-start.20 = (f32[3,256]{1,0:T(4,128)S(1)}, f32[3,256]{1,0:T(4,128)}, u32[]{:S(2)}) copy-start(f32[3,256]{1,0:T(4,128)} %param.16) | copy-start | bytes 9220
  6.5 8.0 %copy-start.21 = (f32[3,256]{1,0:T(4,128)S(1)}, f32[3,256]{1,0:T(4,128)}, u32[]{:S(2)}) copy-start(f32[3,256]{1,0:T(4,128)} %param.17) | copy-start | bytes 9220
  6.5 8.6 %copy-start.7 = (f32[3,31,256]{2,1,0:T(8,128)S(1)}, f32[3,31,256]{2,1,0:T(8,128)}, u32[]{:S(2)}) copy-start(f32[3,31,256]{2,1,0:T(8,128)} %param.15) | copy-start | bytes 285700
  6.5 32.2 %all-gather.13.cloned.1.call-start = ((), (), s32[]{:S(2)}) async-start(), calls=%async_computation.8 | async-start | bytes 3538944 | tf_op jit(solution)/shard_map/all_gather | solution.py:67
  7.3 123.3 %all-gather.9.cloned.1.call-start = ((), (), s32[]{:S(2)}) async-start(), calls=%async_computation.6 | async-start | bytes 13369344 | tf_op jit(solution)/shard_map/all_gather | solution.py:15
  9.5 184.3 %all-gather.11.cloned.1.call-start = ((), (), s32[]{:S(2)}) async-start(), calls=%async_computation.7 | async-start | bytes 6684672 | tf_op jit(solution)/shard_map/all_gather | solution.py:63
  10.3 7.6 %collective-permute-start = (s32[30]{0:T(128)S(1)}, s32[30]{0:T(128)S(1)}, u32[]{:S(2)}, u32[]{:S(2)}) collective-permute-start(s32[30]{0:T(128)S(1)} %slice.999), channel_id=1, source_target_pairs={{0,8},{8,16},{16,24},{24,32},{32,40},{40,48},{48,56},{56,64},{64,7... | collective-permute-start | bytes 368 | tf_op jit(solution)/shard_map/ppermute | solution.py:21
  38.7 2.8 copy-start
  130.6 3.7 copy-start.3
  134.3 10.6 %copy-start.10 = (f32[1,1,256]{2,1,0:T(1,128)S(1)}, f32[1,1,256]{2,1,0:T(1,128)}, u32[]{:S(2)}) copy-start(f32[1,1,256]{2,1,0:T(1,128)} %get-tuple-element.89) | copy-start | bytes 3076
  134.3 10.6 %copy-start.11 = (f32[1,1,256]{2,1,0:T(1,128)S(1)}, f32[1,1,256]{2,1,0:T(1,128)}, u32[]{:S(2)}) copy-start(f32[1,1,256]{2,1,0:T(1,128)} %get-tuple-element.90) | copy-start | bytes 3076
  134.3 10.6 %copy-start.12 = (f32[1,1,256]{2,1,0:T(1,128)S(1)}, f32[1,1,256]{2,1,0:T(1,128)}, u32[]{:S(2)}) copy-start(f32[1,1,256]{2,1,0:T(1,128)} %get-tuple-element.91) | copy-start | bytes 3076
  134.3 10.6 %copy-start.13 = (f32[1,1,256]{2,1,0:T(1,128)S(1)}, f32[1,1,256]{2,1,0:T(1,128)}, u32[]{:S(2)}) copy-start(f32[1,1,256]{2,1,0:T(1,128)} %get-tuple-element.92) | copy-start | bytes 3076
  134.4 10.6 %copy-start.19 = (f32[1,256]{1,0:T(1,128)S(1)}, f32[1,256]{1,0:T(1,128)}, u32[]{:S(2)}) copy-start(f32[1,256]{1,0:T(1,128)} %get-tuple-element.119) | copy-start | bytes 3076
  137.0 7.8 %collective-permute-start.1 = (bf16[30,256]{1,0:T(8,128)(2,1)S(1)}, bf16[30,256]{1,0:T(8,128)(2,1)S(1)}, u32[]{:S(2)}, u32[]{:S(2)}) collective-permute-start(bf16[30,256]{1,0:T(8,128)(2,1)S(1)} %slice.1247), channel_id=1, source_target_pairs={{0,8},{8,16},{16,24},{24,32},{32,40},{40,48},{48,56},{56,64},{64,7... | collective-permute-start | bytes 46088 | tf_op jit(solution)/shard_map/ppermute | solution.py:21
  145.0 8.4 %copy-start.22 = (f32[3,256]{1,0:T(4,128)S(1)}, f32[3,256]{1,0:T(4,128)}, u32[]{:S(2)}) copy-start(f32[3,256]{1,0:T(4,128)} %param.18) | copy-start | bytes 9220
  145.0 13.8 %copy-start.18 = (f32[1,256]{1,0:T(1,128)S(1)}, f32[1,256]{1,0:T(1,128)}, u32[]{:S(2)}) copy-start(f32[1,256]{1,0:T(1,128)} %get-tuple-element.113) | copy-start | bytes 3076
  148.4 45.4 %copy-start.4 = (bf16[384,512]{1,0:T(8,128)(2,1)S(1)}, bf16[384,512]{1,0:T(8,128)(2,1)}, u32[]{:S(2)}) copy-start(bf16[384,512]{1,0:T(8,128)(2,1)} %param.10) | copy-start | bytes 1179652
  149.1 9.7 %all-to-all-start = ((f32[8,1,768]{2,1,0:T(1,128)}), f32[8,1,768]{2,1,0:T(1,128)S(1)}, u32[]{:S(2)}, u32[]{:S(2)}) async-start(f32[8,1,768]{2,1,0:T(1,128)} %broadcast_in_dim.604), calls=%async_computation | async-start | bytes 49152 | tf_op jit(solution)/shard_map/all_to_all | solution.py:26
  160.5 33.3 %all-to-all-start.1 = ((bf16[8,384,256]{1,2,0:T(8,128)(2,1)}), bf16[8,384,256]{1,2,0:T(8,128)(2,1)S(1)}, u32[]{:S(2)}, u32[]{:S(2)}) async-start(bf16[8,384,256]{1,2,0:T(8,128)(2,1)} %broadcast_in_dim.605), calls=%async_computation.1 | async-start | bytes 3145728 | tf_op jit(solution)/shard_map/all_to_all | solution.py:26
  164.1 60.7 %all-gather.15.cloned.1.call-start = ((), (), s32[]{:S(2)}) async-start(), calls=%async_computation.9 | async-start | bytes 3538944 | tf_op jit(solution)/shard_map/all_gather | solution.py:67
  197.2 115.2 %all-gather.17.cloned.1.call-start = ((), (), s32[]{:S(2)}) async-start(), calls=%async_computation.10 | async-start | bytes 3538944 | tf_op jit(solution)/shard_map/all_gather | solution.py:67
  224.8 5.6 %copy-start.1 = (bf16[3072,512]{1,0:T(8,128)(2,1)S(1)}, bf16[3072,512]{1,0:T(8,128)(2,1)}, u32[]{:S(2)}) copy-start(bf16[3072,512]{1,0:T(8,128)(2,1)} %all-gather.15.cloned.1.call-done) | copy-start | bytes 9437188
  237.0 10.5 %copy-start.17 = (f32[1,256]{1,0:T(1,128)S(1)}, f32[1,256]{1,0:T(1,128)}, u32[]{:S(2)}) copy-start(f32[1,256]{1,0:T(1,128)} %get-tuple-element.120) | copy-start | bytes 3076
  239.6 7.7 %collective-permute-start.2 = (bf16[30,256]{1,0:T(8,128)(2,1)S(1)}, bf16[30,256]{1,0:T(8,128)(2,1)S(1)}, u32[]{:S(2)}, u32[]{:S(2)}) collective-permute-start(bf16[30,256]{1,0:T(8,128)(2,1)S(1)} %slice.1282), channel_id=1, source_target_pairs={{0,8},{8,16},{16,24},{24,32},{32,40},{40,48},{48,56},{56,64},{64,7... | collective-permute-start | bytes 46088 | tf_op jit(solution)/shard_map/ppermute | solution.py:21
  247.4 11.8 %copy-start.16 = (f32[1,256]{1,0:T(1,128)S(1)}, f32[1,256]{1,0:T(1,128)}, u32[]{:S(2)}) copy-start(f32[1,256]{1,0:T(1,128)} %get-tuple-element.114) | copy-start | bytes 3076
  250.9 32.9 %copy-start.6 = (bf16[384,512]{1,0:T(8,128)(2,1)S(1)}, bf16[384,512]{1,0:T(8,128)(2,1)}, u32[]{:S(2)}) copy-start(bf16[384,512]{1,0:T(8,128)(2,1)} %fusion.18) | copy-start | bytes 1179652
  312.3 5.6 %copy-start.2 = (bf16[3072,512]{1,0:T(8,128)(2,1)S(1)}, bf16[3072,512]{1,0:T(8,128)(2,1)}, u32[]{:S(2)}) copy-start(bf16[3072,512]{1,0:T(8,128)(2,1)} %all-gather.17.cloned.1.call-done) | copy-start | bytes 9437188
  324.5 10.5 %copy-start.15 = (f32[1,256]{1,0:T(1,128)S(1)}, f32[1,256]{1,0:T(1,128)}, u32[]{:S(2)}) copy-start(f32[1,256]{1,0:T(1,128)} %get-tuple-element.118) | copy-start | bytes 3076
  327.2 7.7 %collective-permute-start.3 = (bf16[30,256]{1,0:T(8,128)(2,1)S(1)}, bf16[30,256]{1,0:T(8,128)(2,1)S(1)}, u32[]{:S(2)}, u32[]{:S(2)}) collective-permute-start(bf16[30,256]{1,0:T(8,128)(2,1)S(1)} %slice.1317), channel_id=1, source_target_pairs={{0,8},{8,16},{16,24},{24,32},{32,40},{40,48},{48,56},{56,64},{64,7... | collective-permute-start | bytes 46088 | tf_op jit(solution)/shard_map/ppermute | solution.py:21
  335.0 11.8 %copy-start.14 = (f32[1,256]{1,0:T(1,128)S(1)}, f32[1,256]{1,0:T(1,128)}, u32[]{:S(2)}) copy-start(f32[1,256]{1,0:T(1,128)} %get-tuple-element.112) | copy-start | bytes 3076
  338.4 32.9 %copy-start.5 = (bf16[384,512]{1,0:T(8,128)(2,1)S(1)}, bf16[384,512]{1,0:T(8,128)(2,1)}, u32[]{:S(2)}) copy-start(bf16[384,512]{1,0:T(8,128)(2,1)} %fusion.17) | copy-start | bytes 1179652
Sparse Core Ops, SparseCore 0:
  9.0 29.6 all-gather.12
  40.9 89.6 all-gather.8
  132.7 61.0 all-gather.10
  197.3 27.4 all-gather.14
  287.3 24.9 all-gather.16
